TPU v7x, 32 devices: a whole 2x2x4 slice. The times are simulated.
32 devices in a mesh: sp: 8 (over z, y), tp: 4 (over x, core).
Axes of the slice: x: 2, y: 2, z: 4, core: 2. Of those that a mesh axis runs over, the one named last changes fastest.
Arguments:
- tokens: bfloat16 [4096, 2048], P(('sp', 'tp')), may hold values from -6 to 6
- norm_gain: float32 [2048], replicated, may hold values from 0.25 to 5
- w_query_one: bfloat16 [2048, 512], P(None, 'tp'), may hold values from -0.21875 to 0.21875
- w_query_two: bfloat16 [2048, 512], P(None, 'tp'), may hold values from -0.21875 to 0.21875
- w_key_one: bfloat16 [2048, 512], P(None, 'tp'), may hold values from -0.125 to 0.125
- w_key_two: bfloat16 [2048, 512], P(None, 'tp'), may hold values from -0.125 to 0.125
- w_value: bfloat16 [2048, 1024], P(None, 'tp'), may hold values from -0.125 to 0.125
- mix_lambda: float32 [8], P('tp'), may hold values from 0.3 to 0.8
- head_gain: float32 [128], replicated, may hold values from 0.1 to 1.9
- w_ret_query: bfloat16 [2048, 512], P(None, 'tp'), may hold values from -0.125 to 0.125
- w_ret_key: bfloat16 [2048, 512], P(None, 'tp'), may hold values from -0.125 to 0.125
- w_ret_value: bfloat16 [2048, 1024], P(None, 'tp'), may hold values from -0.125 to 0.125
- retain_log: float32 [8, 4096], P('tp', 'sp'), may hold values from -1 to 0
- init_state: float32 [8, 64, 128], P('tp'), may hold values from -144 to 144
- w_out_diff: bfloat16 [1024, 2048], P('tp'), may hold values from -0.125 to 0.125
- w_out_ret: bfloat16 [1024, 2048], P('tp'), may hold values from -0.125 to 0.125
Outputs:
- mixed: bfloat16 [4096, 2048], P(('sp', 'tp'))
All inputs are finite; a program needn't handle non-finite values.
Results may differ from a plain program's by a relative error of at most 0.015.
The roundings to bfloat16 on the way count: a program that leaves them out, or rounds other values in their place, can miss the bound.
Values may be sent and summed in bfloat16 or wider, within the bound.
No kernel may reach another device: no remote copies, remote signals or barrier semaphores. Data moves between devices by JAX's collectives and lax.ppermute only.
A program may use at most 128 MiB of HBM per device.

v0:
```python
import math
import jax
import jax.numpy as jnp
from jax import lax
from jax.sharding import PartitionSpec as P

BLOCK = 256
NORM_EPS = 1e-06
HEAD_EPS = 1e-05
DIFF_SCALE = 0.8
HIGHEST = lax.Precision.HIGHEST


def prefix(x, axis, join, neutral):
    place = lax.axis_index(axis)
    gathered = jax.tree.map(
        lambda a, kind: lax.all_gather(a.astype(kind), axis), x, (jnp.bfloat16, jnp.bfloat16)
    )
    state = jax.tree.map(lambda a, e: jnp.zeros_like(a) + jnp.asarray(e, a.dtype), x, neutral)

    def one(turn, state):
        return join(
            state,
            jax.tree.map(
                lambda a, own: lax.dynamic_index_in_dim(a, turn, 0, False).astype(own.dtype),
                gathered,
                x,
            ),
        )

    return lax.fori_loop(0, place, one, state)


def head_norm(values):
    return values * lax.rsqrt(jnp.mean(values * values, axis=-1, keepdims=True) + HEAD_EPS)


def soft_update(running, query, keys, values, allowed):
    peak_old, denominator, weighted = running
    scores = jnp.einsum(
        "qhd,khd->hqk", query, keys, preferred_element_type=jnp.float32
    ) * query.shape[-1] ** (-0.5)
    scores = jnp.where(allowed[None], scores, -jnp.inf)
    peak_new = jnp.maximum(peak_old, jnp.max(scores, axis=-1))
    offset = jnp.where(jnp.isinf(peak_new), 0.0, peak_new)
    rescale = jnp.exp(peak_old - offset)
    shifted = jnp.exp(scores - offset[..., None])
    denominator = denominator * rescale + jnp.sum(shifted, axis=-1)
    weighted = weighted * rescale[..., None] + jnp.einsum(
        "hqk,khe->hqe", shifted.astype(jnp.bfloat16), values, preferred_element_type=jnp.float32
    )
    return (peak_new, denominator, weighted)


def on_device(
    tokens,
    norm_gain,
    w_query_one,
    w_query_two,
    w_key_one,
    w_key_two,
    w_value,
    mix_lambda,
    head_gain,
    w_ret_query,
    w_ret_key,
    w_ret_value,
    retain_log,
    init_state,
    w_out_diff,
    w_out_ret,
):
    key_width = w_query_one.shape[1]
    diff_heads = mix_lambda.shape[0]
    head_dim = key_width // diff_heads
    val_dim = head_gain.shape[0]
    value_width = w_value.shape[1]
    ret_heads = init_state.shape[0]
    ret_width = w_ret_query.shape[1]
    floats = tokens.astype(jnp.float32)
    normed = (
        floats * lax.rsqrt(jnp.mean(floats * floats, axis=-1, keepdims=True) + NORM_EPS) * norm_gain
    ).astype(jnp.bfloat16)
    weights = (
        w_query_one,
        w_query_two,
        w_key_one,
        w_key_two,
        w_value,
        w_ret_query,
        w_ret_key,
        w_ret_value,
    )
    portion = lax.all_gather(normed, "tp", axis=0, tiled=True)
    projected = jnp.concatenate(
        [
            jnp.dot(portion, weight, preferred_element_type=jnp.float32).astype(jnp.bfloat16)
            for weight in weights
        ],
        axis=1,
    )
    row_count = projected.shape[0]
    query_one = projected[:, :key_width].reshape(row_count, diff_heads, head_dim)
    query_two = projected[:, key_width : 2 * key_width].reshape(row_count, diff_heads, head_dim)
    key_pack = projected[:, 2 * key_width : 4 * key_width + value_width]
    ret_begin = 4 * key_width + value_width
    ret_query = projected[:, ret_begin : ret_begin + ret_width]
    ret_key = projected[:, ret_begin + ret_width : ret_begin + 2 * ret_width]
    ret_value = projected[:, ret_begin + 2 * ret_width :]
    nblocks = row_count // BLOCK

    def split_blocks(data, size):
        return data.reshape(nblocks, BLOCK, ret_heads, size).transpose(0, 2, 1, 3)

    block_query = split_blocks(ret_query, head_dim)
    block_key = split_blocks(ret_key, head_dim)
    block_value = split_blocks(ret_value, val_dim)
    log_blocks = retain_log.reshape(ret_heads, nblocks, BLOCK).transpose(1, 0, 2)
    sequence_index = jnp.arange(BLOCK, dtype=jnp.int32)
    causal = sequence_index[:, None] >= sequence_index[None, :]

    def ret_step(memory, inputs):
        query, keys, values, logs = inputs
        cumulative = jnp.cumsum(logs, axis=-1)
        gap_log = jnp.where(causal[None], cumulative[:, :, None] - cumulative[:, None, :], -jnp.inf)
        raw = jnp.einsum("hqd,hkd->hqk", query, keys, preferred_element_type=jnp.float32)
        decayed = (raw * head_dim ** (-0.5) * jnp.exp(gap_log)).astype(jnp.bfloat16)
        result = jnp.einsum("hqk,hke->hqe", decayed, values, preferred_element_type=jnp.float32)
        result = result + jnp.einsum(
            "hqd,hde->hqe",
            query.astype(jnp.float32) * jnp.exp(cumulative)[:, :, None],
            memory,
            precision=HIGHEST,
        )
        last_log = cumulative[:, -1:]
        key_scaled = (
            keys.astype(jnp.float32)
            * head_dim ** (-0.5)
            * jnp.exp(last_log - cumulative)[:, :, None]
        ).astype(jnp.bfloat16)
        memory = jnp.exp(last_log)[:, :, None] * memory + jnp.einsum(
            "hkd,hke->hde", key_scaled, values, preferred_element_type=jnp.float32
        )
        return (memory, result)

    zero_state = jnp.zeros((ret_heads, head_dim, val_dim), jnp.float32)
    local_state, local_out = lax.scan(
        ret_step, zero_state, (block_query, block_key, block_value, log_blocks)
    )
    span_log = jnp.sum(retain_log, axis=1)

    def chain_states(first_part, second_part):
        return (
            first_part[0] + second_part[0],
            first_part[1] * jnp.exp(second_part[0])[:, None, None] + second_part[1],
        )

    before_log, before_state = prefix(
        (span_log, local_state), "sp", chain_states, (jnp.zeros_like(span_log), zero_state)
    )
    carried = before_state + jnp.exp(before_log)[:, None, None] * init_state
    span_cumulative = jnp.cumsum(retain_log, axis=1)
    scaled_query = (
        ret_query.astype(jnp.float32).reshape(row_count, ret_heads, head_dim)
        * jnp.exp(span_cumulative).T[:, :, None]
    )
    ret_heads_out = local_out.transpose(1, 0, 2, 3).reshape(
        ret_heads, row_count, val_dim
    ) + jnp.einsum("thd,hde->hte", scaled_query, carried, precision=HIGHEST)
    ret_out = (
        head_norm(ret_heads_out)
        .transpose(1, 0, 2)
        .reshape(row_count, ret_heads * val_dim)
        .astype(jnp.bfloat16)
    )
    place = lax.axis_index("sp")
    query_pos = place * row_count + jnp.arange(row_count, dtype=jnp.int32)
    last_pos = place * row_count + row_count - 1

    def attend(running, key_block, begin_at):
        key_count = key_block.shape[0]
        keys_one = key_block[:, :key_width].reshape(key_count, diff_heads, head_dim)
        keys_two = key_block[:, key_width : 2 * key_width].reshape(key_count, diff_heads, head_dim)
        values = key_block[:, 2 * key_width :].reshape(key_count, diff_heads, val_dim)
        allowed = query_pos[:, None] >= (begin_at + jnp.arange(key_count, dtype=jnp.int32))[None, :]
        return (
            soft_update(running[0], query_one, keys_one, values, allowed),
            soft_update(running[1], query_two, keys_two, values, allowed),
        )

    empty_map = (
        jnp.full((diff_heads, row_count), -jnp.inf, jnp.float32),
        jnp.zeros((diff_heads, row_count), jnp.float32),
        jnp.zeros((diff_heads, row_count, val_dim), jnp.float32),
    )
    portion = lax.all_gather(key_pack, "sp", axis=0, tiled=True)
    key_count = portion.shape[0]
    stride = math.gcd(key_count, 512)

    def one_block(number, inner_state):
        first_pos = number * stride
        key_block = lax.dynamic_slice_in_dim(portion, number * stride, stride, 0)
        return lax.cond(
            first_pos <= last_pos,
            lambda kept: attend(kept, key_block, first_pos),
            lambda kept: kept,
            inner_state,
        )

    softmax_maps = lax.fori_loop(0, key_count // stride, one_block, (empty_map, empty_map))
    first_map, second_map = softmax_maps
    mixed_heads = (
        first_map[2] / first_map[1][..., None]
        - mix_lambda[:, None, None] * second_map[2] / second_map[1][..., None]
    )
    diff_out = (
        (head_norm(mixed_heads) * head_gain * DIFF_SCALE)
        .transpose(1, 0, 2)
        .reshape(row_count, diff_heads * val_dim)
        .astype(jnp.bfloat16)
    )
    return lax.psum_scatter(
        (
            jnp.dot(diff_out, w_out_diff, preferred_element_type=jnp.float32)
            + jnp.dot(ret_out, w_out_ret, preferred_element_type=jnp.float32)
        ).astype(jnp.bfloat16),
        "tp",
        scatter_dimension=0,
        tiled=True,
    )


def solution(mesh):
    in_specs = (
        P(("sp", "tp"), None),
        P(),
        P(None, "tp"),
        P(None, "tp"),
        P(None, "tp"),
        P(None, "tp"),
        P(None, "tp"),
        P("tp"),
        P(),
        P(None, "tp"),
        P(None, "tp"),
        P(None, "tp"),
        P("tp", "sp"),
        P("tp", None, None),
        P("tp", None),
        P("tp", None),
    )
    out_specs = P(("sp", "tp"), None)
    return jax.shard_map(
        on_device, mesh=mesh, in_specs=in_specs, out_specs=out_specs, check_vma=False
    )
```

profile of v0, /device:TPU:0, one launch (start us, length us, event | category | flops | bytes accessed | tf_op | source)
XLA Modules:
  0.0 263.3 jit_solution(5012526148714268753)
XLA Ops:
  6.5 1.3 fusion.56
  7.9 2.0 fusion.58
  11.6 23.1 %all-reduce = bf16[16]{0:T(256)(128)(2,1)S(1)} all-reduce(bf16[16]{0:T(256)(128)(2,1)S(1)} %dynamic-update-slice), channel_id=2, replica_groups=mesh['sp'=8,'tp'=4] {'sp'}, use_global_device_ids=true, to_apply=%add | all-reduce | flops 16 | bytes 64
  34.8 0.7 reshape.224
  37.1 2.8 %convolution_convert_fusion.1 = bf16[512,256]{0,1:T(8,128)(2,1)S(1)} fusion(bf16[512,2048]{1,0:T(8,128)(2,1)} %all-gather.5.cloned.1.call-done, bf16[2048,256]{1,0:T(8,128)(2,1)} %param.30), kind=kOutput, calls=%fused_computation.83 | convolution fusion | flops 537001984 | bytes 3407872 | tf_op jit(solution)/shard_map/dot_general | solution.py:97
  39.9 1.9 convolution_convert_fusion.6
  41.8 0.8 convolution_convert_fusion.7
  42.6 0.8 pad_maximum_fusion
  43.5 1.9 convolution_convert_fusion.2
  45.5 0.7 copy.65
  46.1 2.6 %convolution_convert_fusion = bf16[512,256]{1,0:T(8,128)(2,1)} fusion(bf16[512,2048]{1,0:T(8,128)(2,1)S(1)} %copy-done.2, bf16[2048,256]{1,0:T(8,128)(2,1)} %param.35), kind=kOutput, calls=%fused_computation.82 | convolution fusion | flops 537001984 | bytes 3407872 | tf_op jit(solution)/shard_map/dot_general | solution.py:97
  48.8 1.8 reshape.213
  50.5 1.7 copy.64
  52.2 1.7 convolution_convert_fusion.3
  54.1 0.7 copy.46
  54.8 14.2 %while.51 = (s32[]{:T(128)}, f32[2,64,128]{2,1,0:T(8,128)S(1)}, f32[2,2,256,128]{3,2,1,0:T(8,128)}, f32[2,2,256]{2,1,0:T(2,128)S(1)}, bf16[2,2,256,64]{2,3,1,0:T...) while((s32[]{:T(128)}, f32[2,64,128]{2,1,0:T(8,128)S(1)}, ...), condition=%wide.region_13.14_spmd.clone, body=%wide.region_10.13_spmd.clone.sunk | while | flops 110134280 | bytes 1677136 | solution.py:147
  56.6 1.4 fusion.109
  58.0 2.1 fusion.110
  60.1 0.6 exponential_bitcast_fusion.3
  60.8 1.1 convolution_add_fusion.6
  61.9 0.6 reduce-window.26
  63.7 1.4 fusion.109
  65.1 2.1 fusion.110
  67.3 0.6 exponential_bitcast_fusion.3
  67.9 1.1 convolution_add_fusion.6
  69.0 34.2 %all-gather.1 = bf16[16,64,128]{2,1,0:T(8,128)(2,1)} all-gather(bf16[2,64,128]{2,1,0:T(8,128)(2,1)S(1)} %convert_element_type.128), channel_id=3, replica_groups=mesh['sp'=8,'tp'=4] {'sp'}, dimensions={0}, use_global_device_ids=true | all-gather | bytes 294912 | tf_op jit(solution)/shard_map/all_gather | solution.py:17
  103.5 2.1 copy.47
  105.6 2.3 reshape.215
  107.8 1.8 multiply_reduce_fusion
  109.8 1.5 convolution_convert_fusion.5
  111.3 1.5 convolution_convert_fusion.4
  112.7 7.3 %all-gather.7.cloned.1.call-done = bf16[4096,512]{0,1:T(8,128)(2,1)} async-done(((bf16[512,512]{0,1:T(8,128)(2,1)}), bf16[4096,512]{0,1:T(8,128)(2,1)}) %all-gather.7.cloned.1.call-update) | async-done | bytes 4194320 | tf_op jit(solution)/shard_map/all_gather | solution.py:196
  120.1 0.8 broadcast_in_dim.88
  120.9 0.8 broadcast_in_dim.88.clone
  121.8 12.4 %while.50 = (s32[]{:T(128)}, f32[2,512]{1,0:T(2,128)S(1)}, f32[2,512]{1,0:T(2,128)S(1)}, f32[2,512,128]{2,1,0:T(8,128)}, f32[2,512]{1,0:T(2,128)S(1)}, /*index=5...) while((s32[]{:T(128)}, f32[2,512]{1,0:T(2,128)S(1)}, ...), condition=%wide.region_8.9_spmd.clone, body=%wide.region_1.8_spmd.clone.sunk | while | flops 410797056 | bytes 26628588 | solution.py:210
  121.8 12.0 %conditional.3 = ((f32[2,512]{1,0:T(2,128)S(1)}, f32[2,512]{1,0:T(2,128)S(1)}, f32[2,512,128]{2,1,0:T(8,128)}, f32[2,512]{1,0:T(2,128)S(1)}, f32[2,512]{1,0:T(2,128)S(1)}, /*index=5*/f32[2,512,128]{2,1,0:T(8,128)})) conditional(s32[]{:T(128)} %convert_element_type.180, (f32[2,512]{1,0:T(2,128)S(1)}, f32[2,512]{1,0:T(2,128)S(1)}, ...), branch_computations={%region_2.2_spmd, %region_3.7_spmd} | conditional | flops 410797056 | bytes 26626238 | solution.py:203
  121.8 1.0 fusion.63
  123.1 1.5 fusion.64
  124.7 0.6 fusion.65
  125.3 1.3 copy-done.1
  126.9 1.0 dynamic-slice.2
  127.9 3.1 %convolution_add_fusion = f32[2,512,128]{2,1,0:T(8,128)} fusion(bf16[512,2,128]{0,2,1:T(8,128)(2,1)S(1)} %bitcast.146, f32[2,512,512]{1,2,0:T(8,128)} %copy-done.1, f32[2,512]{1,0:T(2,128)S(1)} %get-tuple-element.549, f32[2,512,128]{2,1,0:T(8,128)} %get-tuple-element.368, f32[2,512]{1,0:T(2,128)S(1)} %get-tuple-element.548), kind=kOutput, calls=%fused_computation.10 | convolution fusion | flops 135528448 | bytes 3416064 | tf_op jit(solution)/shard_map/while/body/eval_jaxpr/cond/branch_1_fun/hqk,khe->hqe/dot_general | solution.py:49
  131.3 2.4 convolution_add_fusion.1
  134.2 1.2 copy.41
  135.4 1.2 copy.42
  137.1 0.7 fusion.66
  138.3 2.1 add_convert_fusion
  140.4 116.3 %reduce-scatter.2.cloned.1.call-done = bf16[128,2048]{1,0:T(8,128)(2,1)} async-done(((bf16[512,2048]{1,0:T(8,128)(2,1)}), bf16[128,2048]{1,0:T(8,128)(2,1)}) %reduce-scatter.2.cloned.1.call-update) | async-done | bytes 524304 | tf_op jit(solution)/shard_map/reduce_scatter | solution.py:222
  (118 shorter events, 8.0 us)
Async XLA Ops:
  6.5 130.5 %copy-start = (bf16[256,2048]{1,0:T(8,128)(2,1)S(1)}, bf16[256,2048]{1,0:T(8,128)(2,1)}, u32[]{:S(2)}) copy-start(bf16[256,2048]{1,0:T(8,128)(2,1)} %param.38) | copy-start | bytes 3145732
  6.5 3.5 %copy-start.16 = (u32[32]{0:T(128)S(1)}, u32[32]{0:T(128)}, u32[]{:S(2)}) copy-start(u32[32]{0:T(128)} %constant.133) | copy-start | bytes 388
  6.5 4.7 %copy-start.10 = (f32[2,512]{1,0:T(2,128)S(1)}, f32[2,512]{1,0:T(2,128)}, u32[]{:S(2)}) copy-start(f32[2,512]{1,0:T(2,128)} %param.36) | copy-start | bytes 12292
  6.5 30.5 %all-gather.5.cloned.1.call-start = ((), (), s32[]{:S(2)}) async-start(), calls=%async_computation.1 | async-start | bytes 2621440 | tf_op jit(solution)/shard_map/all_gather | solution.py:94
  9.9 110.2 %all-gather.7.cloned.1.call-start = ((), (), s32[]{:S(2)}) async-start(), calls=%async_computation.2 | async-start | bytes 4718592 | tf_op jit(solution)/shard_map/all_gather | solution.py:196
  37.1 2.8 %copy-start.2 = (bf16[512,2048]{1,0:T(8,128)(2,1)S(1)}, bf16[512,2048]{1,0:T(8,128)(2,1)}, u32[]{:S(2)}) copy-start(bf16[512,2048]{1,0:T(8,128)(2,1)} %all-gather.5.cloned.1.call-done) | copy-start | bytes 6291460
  39.8 1.9 copy-start.6
  43.5 213.2 %reduce-scatter.2.cloned.1.call-start = ((), (), s32[]{:S(2)}) async-start(), calls=%async_computation.3 | async-start | bytes 2621440 | tf_op jit(solution)/shard_map/reduce_scatter | solution.py:222
  45.4 3.4 %copy-start.3 = (bf16[512,128]{0,1:T(8,128)(2,1)}, bf16[512,128]{0,1:T(8,128)(2,1)S(1)}, u32[]{:S(2)}) copy-start(bf16[512,128]{0,1:T(8,128)(2,1)S(1)} %convolution_convert_fusion.2) | copy-start | bytes 393220
  56.0 0.5 copy-start.13
  63.1 0.5 copy-start.13
  69.0 38.8 %copy-start.4 = (bf16[512,128]{0,1:T(8,128)(2,1)S(1)}, bf16[512,128]{0,1:T(8,128)(2,1)}, u32[]{:S(2)}) copy-start(bf16[512,128]{0,1:T(8,128)(2,1)} %copy-done.3) | copy-start | bytes 393220
  69.0 38.8 %copy-start.11 = (f32[2,64,128]{2,1,0:T(8,128)S(1)}, f32[2,64,128]{2,1,0:T(8,128)}, u32[]{:S(2)}) copy-start(f32[2,64,128]{2,1,0:T(8,128)} %param.37) | copy-start | bytes 196612
  69.0 38.8 %copy-start.12 = (f32[1,2,4,128]{3,1,2,0:T(2,128)S(1)}, f32[1,2,4,128]{3,1,2,0:T(2,128)}, u32[]{:S(2)}) copy-start(f32[1,2,4,128]{3,1,2,0:T(2,128)} %copy.66) | copy-start | bytes 12292
  107.8 1.9 copy-start.7
  109.7 1.6 copy-start.8
  121.8 2.8 %copy-start.9 = (bf16[512,2,64]{0,2,1:T(8,128)(2,1)S(1)}, bf16[512,2,64]{0,2,1:T(8,128)(2,1)}, u32[]{:S(2)}) copy-start(bf16[512,2,64]{0,2,1:T(8,128)(2,1)} %get-tuple-element.366) | copy-start | bytes 393220 | tf_op jit(solution)/shard_map/while/body/eval_jaxpr/cond
  125.3 1.3 copy-start.1
  134.2 2.5 copy-start.14
  134.2 2.7 %copy-start.15 = (f32[128]{0:T(128)S(1)}, f32[128]{0:T(128)}, u32[]{:S(2)}) copy-start(f32[128]{0:T(128)} %param.32) | copy-start | bytes 1540
  137.0 1.2 copy-start.5
Sparse Core Ops, SparseCore 0:
  10.0 25.2 all-gather.4
  43.6 76.4 all-gather.6
  140.5 116.1 reduce-scatter.1
where the time goes:
time: 266 us; the launch traced here: 263 us
  waiting for transfers between devices  124 us (47%)
  blocking collectives  57.4 us (22%)
  matrix products  36.4 us (14%)
  local copies, waits for them, and re-layouts  22.5 us (8%)
  between operations  14.1 us (5%)
  other arithmetic  8.35 us (3%)
    reduce_scatter x1, waiting for transfers between devices, on_device(): lax.psum_scatter((jnp.dot(diff_out, w_out_diff, preferred_element_type=jn...  116 us
    all_gather x1, blocking collectives, prefix(): lax.all_gather(a.astype(kind), axis)  34.2 us
    unnamed x1, blocking collectives  23.1 us
    dot_general x8, matrix products, on_device(): jnp.dot(portion, weight, preferred_element_type=jnp.float32)  14.7 us
    all_gather x1, waiting for transfers between devices, on_device(): portion = lax.all_gather(key_pack, 'sp', axis=0, tiled=True)  7.34 us
    dot_general x2, matrix products, soft_update(): jnp.einsum('hqk,khe->hqe', shifted.astype(jnp.bfloat16), values, preferre...  5.55 us
  transfers between devices with their start and end apart: 3, of which 2 were waited for; matrix products, arithmetic and copies ran while one was open for 14% of the time, Pallas kernels for 0%

commit v1 on v0

--- a/solution.py
+++ b/solution.py
@@ -1,3 +1,4 @@
+import functools
 import math
 import jax
 import jax.numpy as jnp
@@ -9,6 +10,15 @@
 HEAD_EPS = 1e-05
 DIFF_SCALE = 0.8
 HIGHEST = lax.Precision.HIGHEST
+
+
+def _post_target(message, dev_axis):
+    g_now = jnp.stack([message for _ in range(lax.axis_size(dev_axis))], 0)
+    answer = lax.all_to_all(g_now, axis_name=dev_axis, concat_axis=0, split_axis=0)
+    return jnp.concatenate(answer, axis=0)
+
+
+define_the_pools = functools.partial(_post_target, dev_axis="sp")
 
 
 def prefix(x, axis, join, neutral):
@@ -193,7 +203,7 @@
         jnp.zeros((diff_heads, row_count), jnp.float32),
         jnp.zeros((diff_heads, row_count, val_dim), jnp.float32),
     )
-    portion = lax.all_gather(key_pack, "sp", axis=0, tiled=True)
+    portion = define_the_pools(key_pack)
     key_count = portion.shape[0]
     stride = math.gcd(key_count, 512)
 

time: 266 us -> 281 us (1.056)
  blocking collectives: 57.4 us -> 107 us
  waiting for transfers between devices: 124 us -> 79.4 us
  local copies, waits for them, and re-layouts: 22.5 us -> 34.5 us
  matrix products: 36.4 us -> 31 us
  starting transfers between devices: 0.09 us -> 4.59 us
    all_gather x1, blocking collectives: 34.2 us -> 83.6 us  [prefix(): lax.all_gather(a.astype(kind), axis)]
    reduce_scatter x1, waiting for transfers between devices: 116 us -> 79.4 us  [on_device(): lax.psum_scatter((jnp.dot(diff_out, w_out_diff, preferred_element_type=jn...]
    unnamed x33 -> x36, local copies, waits for them, and re-layouts: 2.66 us -> 10.3 us
    all_gather x1 -> x0, waiting for transfers between devices: 7.34 us -> none  [on_device(): portion = lax.all_gather(key_pack, 'sp', axis=0, tiled=True)]
    all_to_all x0 -> x1, local copies, waits for them, and re-layouts: none -> 6.47 us  [_post_target(): lax.all_to_all(g_now, axis_name=dev_axis, concat_axis=0, split_axis=0)]
    all_to_all x0 -> x1, starting transfers between devices: none -> 4.54 us  [_post_target(): lax.all_to_all(g_now, axis_name=dev_axis, concat_axis=0, split_axis=0)]
    dot_general x2, matrix products: 5.55 us -> 1.42 us  [soft_update(): jnp.einsum('hqk,khe->hqe', shifted.astype(jnp.bfloat16), values, preferre...]
  transfers between devices with their start and end apart: 3 -> 3, of which waited for: 2 -> 1; matrix products, arithmetic and copies ran while one was open for 14% -> 14% of each run, Pallas kernels for 0% -> 0%
where the time goes in v1:
time: 281 us; the launch traced here: 279 us
  blocking collectives  107 us (38%)
  waiting for transfers between devices  79.4 us (28%)
  local copies, waits for them, and re-layouts  34.5 us (12%)
  matrix products  31 us (11%)
  between operations  14.4 us (5%)
  other arithmetic  7.59 us (3%)
  starting transfers between devices  4.59 us (2%)
    all_gather x1, blocking collectives, prefix(): lax.all_gather(a.astype(kind), axis)  83.6 us
    reduce_scatter x1, waiting for transfers between devices, on_device(): lax.psum_scatter((jnp.dot(diff_out, w_out_diff, preferred_element_type=jn...  79.4 us
    unnamed x1, blocking collectives  23.1 us
    dot_general x8, matrix products, on_device(): jnp.dot(portion, weight, preferred_element_type=jnp.float32)  14.5 us
    unnamed x36, local copies, waits for them, and re-layouts  10.3 us
    all_to_all x1, local copies, waits for them, and re-layouts, _post_target(): lax.all_to_all(g_now, axis_name=dev_axis, concat_axis=0, split_axis=0)  6.47 us
  transfers between devices with their start and end apart: 3, of which 1 were waited for; matrix products, arithmetic and copies ran while one was open for 14% of the time, Pallas kernels for 0%

profile of v1, /device:TPU:0, one launch (start us, length us, event | category | flops | bytes accessed | tf_op | source)
XLA Modules:
  0.0 279.1 jit_solution(11218382077896090570)
XLA Ops:
  6.5 1.3 fusion.56
  7.9 2.0 fusion.58
  11.6 23.1 %all-reduce = bf16[16]{0:T(256)(128)(2,1)S(1)} all-reduce(bf16[16]{0:T(256)(128)(2,1)S(1)} %dynamic-update-slice), channel_id=2, replica_groups=mesh['sp'=8,'tp'=4] {'sp'}, use_global_device_ids=true, to_apply=%add | all-reduce | flops 16 | bytes 64
  34.7 0.7 reshape.230
  35.4 0.6 reduce-window.16
  36.4 0.6 copy.80
  37.1 2.6 convolution_convert_fusion.6
  39.7 1.9 convolution_convert_fusion.7
  41.6 0.8 convolution_convert_fusion.1
  42.4 2.3 stack.2
  44.8 4.5 %all-to-all-start = ((bf16[8,512,512]{1,2,0:T(8,128)(2,1)}), bf16[8,512,512]{1,2,0:T(8,128)(2,1)}, u32[]{:S(2)}, u32[]{:S(2)}) async-start(bf16[8,512,512]{1,2,0:T(8,128)(2,1)} %stack.2), calls=%async_computation | async-start | bytes 8388608 | tf_op jit(solution)/shard_map/all_to_all | solution.py:17
  49.4 1.9 convolution_convert_fusion.2
  51.3 0.7 copy.79
  51.9 2.4 convolution_convert_fusion.3
  54.3 1.0 copy.57
  55.4 0.7 reshape.218
  56.1 1.6 copy.60
  57.6 2.6 convolution_convert_fusion
  60.3 1.7 reshape.219
  62.0 1.7 copy.78
  63.7 13.0 %while.51 = (s32[]{:T(128)}, f32[2,64,128]{2,1,0:T(8,128)S(1)}, f32[2,2,256,128]{3,2,1,0:T(8,128)}, f32[2,2,256]{2,1,0:T(2,128)S(1)}, bf16[2,2,256,64]{2,3,1,0:T...) while((s32[]{:T(128)}, f32[2,64,128]{2,1,0:T(8,128)S(1)}, ...), condition=%wide.region_13.14_spmd.clone, body=%wide.region_10.13_spmd.clone.sunk | while | flops 110134280 | bytes 1678610 | solution.py:157
  63.7 0.6 reduce-window.26
  65.6 1.4 fusion.109
  67.0 2.2 fusion.110
  69.1 1.1 convolution_add_fusion.6
  70.2 0.6 reduce-window.26
  72.1 1.4 fusion.109
  73.5 2.1 fusion.110
  75.7 1.1 convolution_add_fusion.6
  76.8 2.1 copy.61
  78.9 2.3 reshape.221
  81.2 83.6 %all-gather.1 = bf16[16,64,128]{2,1,0:T(8,128)(2,1)} all-gather(bf16[2,64,128]{2,1,0:T(8,128)(2,1)S(1)} %convert_element_type.128), channel_id=3, replica_groups=mesh['sp'=8,'tp'=4] {'sp'}, dimensions={0}, use_global_device_ids=true | all-gather | bytes 294912 | tf_op jit(solution)/shard_map/all_gather | solution.py:27
  165.0 1.8 multiply_reduce_fusion
  167.0 0.8 convolution_convert_fusion.4
  167.9 1.5 convolution_convert_fusion.5
  169.4 6.5 %copy.53 = bf16[8,512,512]{2,1,0:T(8,128)(2,1)} copy(bf16[8,512,512]{1,2,0:T(8,128)(2,1)} %all-to-all-done) | data formatting | bytes 8388608 | tf_op jit(solution)/shard_map/all_to_all | solution.py:17
  175.9 6.4 %copy.54 = bf16[4096,512]{0,1:T(8,128)(2,1)} copy(bf16[4096,512]{1,0:T(8,128)(2,1)} %bitcast.149) | data formatting | bytes 8388608
  182.4 6.1 %while.50 = (s32[]{:T(128)}, f32[2,512]{1,0:T(2,128)S(1)}, f32[2,512]{1,0:T(2,128)S(1)}, f32[2,512,128]{2,1,0:T(8,128)S(1)}, f32[2,512]{1,0:T(2,128)S(1)}, /*ind...) while((s32[]{:T(128)}, f32[2,512]{1,0:T(2,128)S(1)}, ...), condition=%wide.region_8.9_spmd.clone, body=%wide.region_1.8_spmd.clone.sunk | while | flops 410797056 | bytes 17715636 | solution.py:220
  182.5 5.6 %conditional.3 = ((f32[2,512]{1,0:T(2,128)S(1)}, f32[2,512]{1,0:T(2,128)S(1)}, f32[2,512,128]{2,1,0:T(8,128)S(1)}, f32[2,512]{1,0:T(2,128)S(1)}, f32[2,512]{1,0:T(2,128)S(1)}, /*index=5*/f32[2,512,128]{2,1,0:T(8,128)S(1)})) conditional(s32[]{:T(128)} %convert_element_type.180, (f32[2,512]{1,0:T(2,128)S(1)}, f32[2,512]{1,0:T(2,128)S(1)}, ...), branch_computations={%region_2.2_spmd, %region_3.7_spmd} | conditional | flops 410797056 | bytes 17713286 | solution.py:213
  182.7 1.0 dynamic-slice.2
  183.7 1.0 fusion.63
  184.7 0.6 fusion.64
  185.4 0.6 fusion.65
  186.6 0.7 convolution_add_fusion.1
  187.4 0.7 convolution_add_fusion
  189.6 0.7 fusion.66
  190.8 2.1 add_convert_fusion
  192.9 79.4 %reduce-scatter.2.cloned.1.call-done = bf16[128,2048]{1,0:T(8,128)(2,1)} async-done(((bf16[512,2048]{1,0:T(8,128)(2,1)}), bf16[128,2048]{1,0:T(8,128)(2,1)}) %reduce-scatter.2.cloned.1.call-update) | async-done | bytes 524304 | tf_op jit(solution)/shard_map/reduce_scatter | solution.py:232
  (114 shorter events, 7.0 us)
Async XLA Ops:
  6.5 183.0 %copy-start = (bf16[256,2048]{1,0:T(8,128)(2,1)S(1)}, bf16[256,2048]{1,0:T(8,128)(2,1)}, u32[]{:S(2)}) copy-start(bf16[256,2048]{1,0:T(8,128)(2,1)} %param.38) | copy-start | bytes 3145732
  6.5 3.6 %copy-start.14 = (u32[32]{0:T(128)S(1)}, u32[32]{0:T(128)}, u32[]{:S(2)}) copy-start(u32[32]{0:T(128)} %constant.133) | copy-start | bytes 388
  6.5 3.4 %copy-start.8 = (f32[2,512]{1,0:T(2,128)S(1)}, f32[2,512]{1,0:T(2,128)}, u32[]{:S(2)}) copy-start(f32[2,512]{1,0:T(2,128)} %param.36) | copy-start | bytes 12292
  6.5 30.5 %all-gather.4.cloned.1.call-start = ((), (), s32[]{:S(2)}) async-start(), calls=%async_computation.2 | async-start | bytes 2621440 | tf_op jit(solution)/shard_map/all_gather | solution.py:104
  37.0 2.7 copy-start.1
  37.1 4.5 %copy-start.13 = (bf16[2048,256]{1,0:T(8,128)(2,1)S(1)}, bf16[2048,256]{1,0:T(8,128)(2,1)}, u32[]{:S(2)}) copy-start(bf16[2048,256]{1,0:T(8,128)(2,1)} %param.30) | copy-start | bytes 3145732
  44.8 124.7 %all-to-all-start = ((bf16[8,512,512]{1,2,0:T(8,128)(2,1)}), bf16[8,512,512]{1,2,0:T(8,128)(2,1)}, u32[]{:S(2)}, u32[]{:S(2)}) async-start(bf16[8,512,512]{1,2,0:T(8,128)(2,1)} %stack.2), calls=%async_computation | async-start | bytes 8388608 | tf_op jit(solution)/shard_map/all_to_all | solution.py:17
  49.3 223.0 %reduce-scatter.2.cloned.1.call-start = ((), (), s32[]{:S(2)}) async-start(), calls=%async_computation.3 | async-start | bytes 2621440 | tf_op jit(solution)/shard_map/reduce_scatter | solution.py:232
  51.2 9.0 %copy-start.2 = (bf16[512,128]{0,1:T(8,128)(2,1)}, bf16[512,128]{0,1:T(8,128)(2,1)S(1)}, u32[]{:S(2)}) copy-start(bf16[512,128]{0,1:T(8,128)(2,1)S(1)} %convolution_convert_fusion.2) | copy-start | bytes 393220
  76.7 88.3 %copy-start.3 = (bf16[512,128]{0,1:T(8,128)(2,1)S(1)}, bf16[512,128]{0,1:T(8,128)(2,1)}, u32[]{:S(2)}) copy-start(bf16[512,128]{0,1:T(8,128)(2,1)} %copy-done.2) | copy-start | bytes 393220
  76.8 88.3 %copy-start.9 = (f32[2,64,128]{2,1,0:T(8,128)S(1)}, f32[2,64,128]{2,1,0:T(8,128)}, u32[]{:S(2)}) copy-start(f32[2,64,128]{2,1,0:T(8,128)} %param.37) | copy-start | bytes 196612
  76.8 88.3 %copy-start.10 = (f32[1,2,4,128]{3,1,2,0:T(2,128)S(1)}, f32[1,2,4,128]{3,1,2,0:T(2,128)}, u32[]{:S(2)}) copy-start(f32[1,2,4,128]{3,1,2,0:T(2,128)} %copy.80) | copy-start | bytes 12292
  165.0 2.0 copy-start.5
  166.9 1.0 copy-start.6
  175.9 6.6 %copy-start.7 = (bf16[512,128]{0,1:T(8,128)(2,1)S(1)}, bf16[512,128]{0,1:T(8,128)(2,1)}, u32[]{:S(2)}) copy-start(bf16[512,128]{0,1:T(8,128)(2,1)} %convolution_convert_fusion.5) | copy-start | bytes 393220
  188.5 0.7 copy-start.11
  188.6 0.9 copy-start.12
  189.5 1.2 copy-start.4
Sparse Core Ops, SparseCore 0:
  10.1 25.2 all-gather.3
  193.0 79.2 reduce-scatter.1
